TPU v7x, 32 devices: a whole 2x2x4 slice. The times are simulated.
32 devices in a mesh: sp: 4 (over z), tp: 4 (over y, x), dp: 2 (over core).
Axes of the slice: x: 2, y: 2, z: 4, core: 2. Of those that a mesh axis runs over, the one named last changes fastest.
Arguments:
- latent: bfloat16 [4, 4096, 2048], P('dp', 'sp'), may hold values from -6 to 6
- context: bfloat16 [4, 1024, 2048], P('dp', 'sp'), may hold values from -6 to 6
- condition: bfloat16 [4, 2048], P('dp', 'sp'), may hold values from -6 to 6
- ctx_cond: bfloat16 [2048], P('sp'), may hold values from -6 to 6
- norm_gain: float32 [2048], replicated, may hold values from 0.1 to 1.9
- w_shift: bfloat16 [2048, 2048], P('sp', 'tp'), may hold values from -0.125 to 0.125
- w_scale: bfloat16 [2048, 2048], P('sp', 'tp'), may hold values from -0.125 to 0.125
- w_gate: bfloat16 [2048, 2048], P('sp', 'tp'), may hold values from -0.125 to 0.125
- w_query: bfloat16 [2048, 1024], P(None, 'tp'), may hold values from -0.125 to 0.125
- w_key: bfloat16 [2048, 256], P(None, 'tp'), may hold values from -0.125 to 0.125
- w_value: bfloat16 [2048, 256], P(None, 'tp'), may hold values from -0.125 to 0.125
- w_out: bfloat16 [1024, 2048], P('tp'), may hold values from -4 to 4
- sink_logit: float32 [16], P('tp'), may hold values from 4 to 7
- ctx_lift: float32 [16], P('tp'), may hold values from -4 to 220
Outputs:
- mixed: bfloat16 [4, 4096, 2048], P('dp', ('sp', 'tp'))
All inputs are finite; a program needn't handle non-finite values.
Results may differ from a plain program's by a relative error of at most 0.012.
Values may be sent and summed in bfloat16 or wider, within the bound.
A program may use at most 128 MiB of HBM per device.

v0:
```python
import jax
import jax.numpy as jnp
from jax import lax
from jax.sharding import PartitionSpec as P

HEAD = 64
WINDOW = 128
GRID_COLS = 64


epsilon = 1e-06
rope_base = 10000.0
masked_value = -1e30


def with_halo(cells, sides, width):
    for axis, dim in sides:
        count = lax.axis_size(axis)
        ends = count - 1
        head = lax.slice_in_dim(cells, 0, width, axis=dim)
        tail = lax.slice_in_dim(cells, cells.shape[dim] - width, cells.shape[dim], axis=dim)
        cells = jnp.concatenate(
            [
                lax.ppermute(tail, axis, [(i, (i + 1) % count) for i in range(ends)]),
                cells,
                lax.ppermute(head, axis, [((i + 1) % count, i) for i in range(ends)]),
            ],
            axis=dim,
        )
    return cells


def modulated(inputs, norm_gain, shift_vec, scale_vec):
    widened = inputs.astype(jnp.float32)
    inverse = lax.rsqrt(jnp.mean(widened * widened, axis=-1, keepdims=True) + epsilon)
    return (widened * inverse * norm_gain * (1.0 + scale_vec) + shift_vec).astype(jnp.bfloat16)


def rotate_half(half_part, angles):
    first_half, second = jnp.split(half_part, 2, axis=-1)
    cosine = jnp.cos(angles)[:, None, :]
    sine_part = jnp.sin(angles)[:, None, :]
    return jnp.concatenate(
        [first_half * cosine - second * sine_part, first_half * sine_part + second * cosine],
        axis=-1,
    )


def rotate(inputs, positions):
    quarter = inputs.shape[-1] // 4
    frequency = rope_base ** (-jnp.arange(quarter, dtype=jnp.float32) / quarter)
    row_angle = (positions // GRID_COLS).astype(jnp.float32)[:, None] * frequency
    col_angle = (positions % GRID_COLS).astype(jnp.float32)[:, None] * frequency
    half_size = 2 * quarter
    return jnp.concatenate(
        [
            rotate_half(inputs[..., :half_size], row_angle),
            rotate_half(inputs[..., half_size:], col_angle),
        ],
        axis=-1,
    )


def shards(
    latent,
    context,
    condition,
    ctx_cond,
    norm_gain,
    w_shift,
    w_scale,
    w_gate,
    w_query,
    w_key,
    w_value,
    w_out,
    sink_logit,
    ctx_lift,
):
    samples, tokens, model_width = latent.shape
    head_size = HEAD
    sp_count = lax.axis_size("sp")
    cond_rows = jnp.concatenate([condition, ctx_cond[None, :]], axis=0)
    active = jax.nn.silu(cond_rows.astype(jnp.float32)).astype(jnp.bfloat16)
    shift_part, scale_part, gate_part = lax.psum(
        (
            jnp.dot(active, w_shift, preferred_element_type=jnp.float32),
            jnp.dot(active, w_scale, preferred_element_type=jnp.float32),
            jnp.dot(active, w_gate, preferred_element_type=jnp.float32),
        ),
        "sp",
    )
    shift_vec, scale_vec, gate_vec = (
        lax.all_gather(shift_part, "tp", axis=1, tiled=True),
        lax.all_gather(scale_part, "tp", axis=1, tiled=True),
        lax.all_gather(gate_part, "tp", axis=1, tiled=True),
    )
    hidden = modulated(
        latent, norm_gain, shift_vec[:samples, None, :], scale_vec[:samples, None, :]
    )
    offset_row = lax.axis_index("sp") * tokens
    positions = offset_row + jnp.arange(tokens, dtype=jnp.int32)
    query_heads = w_query.shape[1] // head_size
    key_heads = w_key.shape[1] // head_size
    group_size = query_heads // key_heads
    keyed = key_heads * head_size
    queries = rotate(
        jnp.einsum("snd,dc->snc", hidden, w_query, preferred_element_type=jnp.float32).reshape(
            samples, tokens, query_heads, head_size
        ),
        positions,
    ).astype(jnp.bfloat16)
    key_rows = rotate(
        jnp.einsum("snd,dc->snc", hidden, w_key, preferred_element_type=jnp.float32).reshape(
            samples, tokens, key_heads, head_size
        ),
        positions,
    ).astype(jnp.bfloat16)
    values = jnp.einsum("snd,dc->snc", hidden, w_value, preferred_element_type=jnp.float32).astype(
        jnp.bfloat16
    )
    local_pairs = jnp.concatenate([key_rows.reshape(samples, tokens, keyed), values], axis=-1)
    extended = with_halo(local_pairs, (("sp", 1),), WINDOW)
    ctx_hidden = modulated(context, norm_gain, shift_vec[samples], scale_vec[samples])
    ctx_keys = jnp.einsum(
        "snd,dc->snc", ctx_hidden, w_key, preferred_element_type=jnp.float32
    ).astype(jnp.bfloat16)
    ctx_values = jnp.einsum(
        "snd,dc->snc", ctx_hidden, w_value, preferred_element_type=jnp.float32
    ).astype(jnp.bfloat16)
    context_pairs = lax.all_gather(
        jnp.concatenate([ctx_keys, ctx_values], axis=-1), "sp", axis=1, tiled=True
    )
    block_rows = min(512, tokens)
    blocks = tokens // block_rows
    span_rows = block_rows + 2 * WINDOW
    latent_len = tokens * sp_count
    lift_rows = ctx_lift.reshape(key_heads, group_size, 1, 1)
    sink_rows = sink_logit.reshape(key_heads, group_size, 1, 1)
    factor = head_size ** (-0.5)

    def attend(step_id):
        sample = step_id // blocks
        row_start = step_id % blocks * block_rows
        q_rows = lax.dynamic_slice_in_dim(
            lax.dynamic_index_in_dim(queries, sample, 0, keepdims=False), row_start, block_rows, 0
        )
        q_rows = q_rows.reshape(block_rows, key_heads, group_size, head_size)
        pair_rows = lax.dynamic_slice_in_dim(
            lax.dynamic_index_in_dim(extended, sample, 0, keepdims=False), row_start, span_rows, 0
        )
        near_keys = pair_rows[:, :keyed].reshape(span_rows, key_heads, head_size)
        near_values = pair_rows[:, keyed:].reshape(span_rows, key_heads, head_size)
        ctx_rows = lax.dynamic_index_in_dim(context_pairs, sample, 0, keepdims=False)
        far_keys = ctx_rows[:, :keyed].reshape(-1, key_heads, head_size)
        far_values = ctx_rows[:, keyed:].reshape(-1, key_heads, head_size)
        query_pos = offset_row + row_start + jnp.arange(block_rows, dtype=jnp.int32)
        key_pos = offset_row + row_start - WINDOW + jnp.arange(span_rows, dtype=jnp.int32)
        inside = (
            (key_pos[None, :] >= 0)
            & (key_pos[None, :] < latent_len)
            & (jnp.abs(query_pos[:, None] - key_pos[None, :]) <= WINDOW)
        )
        near_scores = (
            jnp.einsum("qgrd,kgd->grqk", q_rows, near_keys, preferred_element_type=jnp.float32)
            * factor
        )
        near_scores = jnp.where(inside[None, None], near_scores, masked_value)
        far_scores = (
            jnp.einsum("qgrd,kgd->grqk", q_rows, far_keys, preferred_element_type=jnp.float32)
            * factor
            + lift_rows
        )
        row_max = jnp.maximum(
            jnp.maximum(near_scores.max(-1, keepdims=True), far_scores.max(-1, keepdims=True)),
            sink_rows,
        )
        near_exp = jnp.exp(near_scores - row_max)
        far_exp = jnp.exp(far_scores - row_max)
        normaliser = (
            near_exp.sum(-1, keepdims=True)
            + far_exp.sum(-1, keepdims=True)
            + jnp.exp(sink_rows - row_max)
        )
        outcome = jnp.einsum(
            "grqk,kgd->qgrd",
            (near_exp / normaliser).astype(jnp.bfloat16),
            near_values,
            preferred_element_type=jnp.float32,
        )
        outcome = outcome + jnp.einsum(
            "grqk,kgd->qgrd",
            (far_exp / normaliser).astype(jnp.bfloat16),
            far_values,
            preferred_element_type=jnp.float32,
        )
        return outcome.astype(jnp.bfloat16).reshape(block_rows, query_heads * head_size)

    attended = lax.map(attend, jnp.arange(samples * blocks, dtype=jnp.int32)).reshape(
        samples, tokens, query_heads * head_size
    )
    by_rows = lax.all_to_all(attended, "tp", split_axis=1, concat_axis=2, tiled=True)
    projected = jnp.einsum(
        "snc,cd->snd",
        by_rows,
        lax.all_gather(w_out, "tp", axis=0, tiled=True),
        preferred_element_type=jnp.float32,
    )
    return (gate_vec[:samples, None, :] * projected).astype(jnp.bfloat16)


def solution(mesh):
    return jax.shard_map(
        shards,
        mesh=mesh,
        in_specs=(
            P("dp", "sp", None),
            P("dp", "sp", None),
            P("dp", "sp"),
            P("sp"),
            P(),
            P("sp", "tp"),
            P("sp", "tp"),
            P("sp", "tp"),
            P(None, "tp"),
            P(None, "tp"),
            P(None, "tp"),
            P("tp", None),
            P("tp"),
            P("tp"),
        ),
        out_specs=P("dp", ("sp", "tp"), None),
        check_vma=False,
    )
```

profile of v0, /device:TPU:0, one launch (start us, length us, event | category | flops | bytes accessed | tf_op | source)
XLA Modules:
  0.0 226.5 jit_solution(14336475768110559586)
XLA Ops:
  8.6 1.2 fusion.72
  9.8 1.2 fusion.74
  11.1 21.3 %all-reduce = (f32[3,512]{1,0:T(4,128)S(1)}, f32[3,512]{1,0:T(4,128)S(1)}, f32[3,512]{1,0:T(4,128)}) all-reduce(f32[3,512]{1,0:T(4,128)S(1)} %fusion.70, f32[3,512]{1,0:T(4,128)S(1)} %fusion.72, f32[3,512]{1,0:T(4,128)S(1)} %fusion.74), channel_id=1, replica_groups=mesh['sp'=4,'tp'=4,'dp'=2] {'sp'}, use_global_device_ids=true, to_apply=%region_3.4 | all-reduce | flops 4608 | bytes 36864 | tf_op jit(solution)/shard_map/psum | solution.py:85
  32.3 8.2 %all_gather.17 = f32[3,2048]{1,0:T(4,128)S(1)} all-gather(f32[3,512]{1,0:T(4,128)S(1)} %get-tuple-element.178), channel_id=1, replica_groups=mesh['sp'=4,'tp'=4,'dp'=2] {'tp'}, dimensions={1}, use_global_device_ids=true | all-gather | bytes 30720 | tf_op jit(solution)/shard_map/all_gather | solution.py:94
  40.5 8.2 %all_gather.16 = f32[3,2048]{1,0:T(4,128)S(1)} all-gather(f32[3,512]{1,0:T(4,128)S(1)} %get-tuple-element.179), channel_id=1, replica_groups=mesh['sp'=4,'tp'=4,'dp'=2] {'tp'}, dimensions={1}, use_global_device_ids=true | all-gather | bytes 30720 | tf_op jit(solution)/shard_map/all_gather | solution.py:95
  48.7 5.1 %fusion.26 = f32[2,1024]{1,0:T(2,128)S(1)} fusion(bf16[2,1024,2048]{2,1,0:T(8,128)(2,1)} %param.16), kind=kLoop, calls=%fused_computation.44 | loop fusion | flops 12580864 | bytes 8396800 | tf_op jit(solution)/shard_map/reduce_sum | solution.py:35
  54.4 6.0 %convolution_bitcast_fusion = f32[2,1024,1,64]{1,3,0,2:T(8,128)S(1)} fusion(bf16[2,1024,2048]{2,1,0:T(8,128)(2,1)} %param.16, f32[2,2048]{1,0:T(2,128)S(1)} %slice.74, f32[2,2048]{1,0:T(2,128)S(1)} %slice_add_fusion, f32[2048]{0:T(1024)S(1)} %copy-done.6, f32[2,1024]{1,0:T(2,128)S(1)} %add_rsqrt_fusion, bf16[2048,64]{0,1:T(8,128)(2,1)S(1)} %copy-done.5), kind=kOutput, calls=%fused_computation.59 | convolution fusion | flops 562036736 | bytes 9224192 | tf_op jit(solution)/shard_map/snd,dc->snc/dot_general | solution.py:114
  60.5 6.9 %fusion.40 = bf16[2,1024,128]{1,2,0:T(8,128)(2,1)S(1)} fusion(bf16[2,1024,128]{1,2,0:T(8,128)(2,1)S(1)} %fusion.59, bf16[2,1024,2048]{2,1,0:T(8,128)(2,1)} %param.16, f32[2,2048]{1,0:T(2,128)S(1)} %slice.74, f32[2,2048]{1,0:T(2,128)S(1)} %slice_add_fusion, f32[2048]{0:T(1024)S(1)} %copy-done.6, f32[2,1024]{1,0:T(2,128)S(1)} %add_rsqrt_fusion, ...), kind=kOutput, calls=%fused_computation.61 | convolution fusion | flops 562167808 | bytes 8962048 | tf_op jit(solution)/shard_map/snd,dc->snc/dot_general | solution.py:119
  67.5 1.3 collective-permute-start
  68.8 1.5 collective-permute-start.1
  70.4 2.1 fusion.31
  72.4 2.6 %convolution_convert_fusion.1 = bf16[2,256,64]{1,2,0:T(8,128)(2,1)S(1)} fusion(bf16[2,256,2048]{2,1,0:T(8,128)(2,1)} %param.17, f32[2048]{0:T(1024)S(1)} %bitcast.202, f32[2048]{0:T(1024)S(1)} %bitcast.200, f32[2048]{0:T(1024)S(1)} %copy-done.6, f32[2,256]{1,0:T(2,128)S(1)} %add_rsqrt_fusion.1, bf16[2048,64]{0,1:T(8,128)(2,1)S(1)} %copy-done.4), kind=kOutput, calls=%fused_computation.62 | convolution fusion | flops 140541952 | bytes 2451456 | tf_op jit(solution)/shard_map/snd,dc->snc/dot_general | solution.py:128
  75.1 2.6 %convolution_convert_fusion.2 = bf16[2,256,64]{1,2,0:T(8,128)(2,1)S(1)} fusion(bf16[2,256,2048]{2,1,0:T(8,128)(2,1)} %param.17, f32[2048]{0:T(1024)S(1)} %bitcast.203, f32[2048]{0:T(1024)S(1)} %bitcast.201, f32[2048]{0:T(1024)S(1)} %copy-done.6, f32[2,256]{1,0:T(2,128)S(1)} %add_rsqrt_fusion.1, bf16[2048,64]{0,1:T(8,128)(2,1)S(1)} %copy-done.5), kind=kOutput, calls=%fused_computation.63 | convolution fusion | flops 140541952 | bytes 2451456 | tf_op jit(solution)/shard_map/snd,dc->snc/dot_general | solution.py:125
  77.7 6.7 %fusion.43 = f32[2,1024,256]{1,2,0:T(8,128)S(1)} fusion(bf16[2048,256]{1,0:T(8,128)(2,1)S(1)} %copy-done, bf16[2,1024,2048]{2,1,0:T(8,128)(2,1)} %param.16, f32[2,2048]{1,0:T(2,128)S(1)} %slice.74, f32[2,2048]{1,0:T(2,128)S(1)} %slice_add_fusion, f32[2048]{0:T(1024)S(1)} %copy-done.6, f32[2,1024]{1,0:T(2,128)S(1)} %add_rsqrt_fusion), kind=kOutput, calls=%fused_computation.65 | convolution fusion | flops 2172649472 | bytes 11583488 | tf_op jit(solution)/shard_map/snd,dc->snc/dot_general | solution.py:108
  84.8 15.8 %all_gather.18 = bf16[2,1024,128]{1,2,0:T(8,128)(2,1)S(1)} all-gather(bf16[2,256,128]{1,2,0:T(8,128)(2,1)S(1)} %pad_maximum_fusion.2), channel_id=1, replica_groups=mesh['sp'=4,'tp'=4,'dp'=2] {'sp'}, dimensions={1}, use_global_device_ids=true | all-gather | bytes 655360 | tf_op jit(solution)/shard_map/all_gather | solution.py:131
  102.2 91.8 %while.13 = (s32[]{:T(128)}, bf16[4,512,256]{2,1,0:T(8,128)(2,1)}, s32[4]{0:T(128)}, bf16[2,1280,128]{1,2,0:T(8,128)(2,1)}, s32[]{:T(128)}, /*index=5*/bf16[2,10...) while((s32[]{:T(128)}, bf16[4,512,256]{2,1,0:T(8,128)(2,1)}, ...), condition=%wide.region_10.11_spmd, body=%wide.region_5.10_spmd.sunk | while | flops 985405696 | bytes 75191968 | solution.py:199
  102.2 1.3 dynamic_slice.51
  105.8 4.6 %bitcast_reduce_fusion.2 = (f32[4,512]{1,0:T(4,128)S(1)}, f32[1024,512,4]{1,0,2:T(8,128)}) fusion(f32[4]{0:T(128)S(1)} %bitcast.194, bf16[2,1024,4,64]{1,3,2,0:T(8,128)(2,1)S(1)} %get-tuple-element.303, s32[]{:T(128)S(6)} %select_n.121, s32[]{:T(128)S(6)} %select_n.124, bf16[1024,128]{0,1:T(8,128)(2,1)S(1)} %dynamic-slice_bitcast_fusion.4), kind=kOutput, calls=%fused_computation.1.clone.1 | convolution fusion | flops 274724864 | bytes 8790536 | tf_op jit(solution)/shard_map/while/body/eval_jaxpr/qgrd,kgd->grqk/dot_general | solution.py:170
  112.0 1.3 fusion.92
  113.4 5.2 %fusion.94 = f32[4,512]{1,0:T(4,128)S(1)} fusion(f32[1024,512,4]{1,0,2:T(8,128)} %get-tuple-element.260, f32[4,512]{1,0:T(4,128)S(1)} %maximum_maximum_fusion.2, f32[4]{0:T(128)S(1)} %bitcast.195), kind=kLoop, calls=%fused_computation.5.clone.1 | loop fusion | flops 8386560 | bytes 8405008 | tf_op jit(solution)/shard_map/while/body/eval_jaxpr/reduce_sum | solution.py:182
  118.7 1.4 fusion.93
  120.2 2.1 fusion.95
  122.3 2.0 fusion.96
  125.2 1.2 dynamic_slice.51
  128.8 4.6 %bitcast_reduce_fusion.2 = (f32[4,512]{1,0:T(4,128)S(1)}, f32[1024,512,4]{1,0,2:T(8,128)}) fusion(f32[4]{0:T(128)S(1)} %bitcast.194, bf16[2,1024,4,64]{1,3,2,0:T(8,128)(2,1)S(1)} %get-tuple-element.303, s32[]{:T(128)S(6)} %select_n.121, s32[]{:T(128)S(6)} %select_n.124, bf16[1024,128]{0,1:T(8,128)(2,1)S(1)} %dynamic-slice_bitcast_fusion.4), kind=kOutput, calls=%fused_computation.1.clone.1 | convolution fusion | flops 274724864 | bytes 8790536 | tf_op jit(solution)/shard_map/while/body/eval_jaxpr/qgrd,kgd->grqk/dot_general | solution.py:170
  135.0 1.3 fusion.92
  136.4 5.2 %fusion.94 = f32[4,512]{1,0:T(4,128)S(1)} fusion(f32[1024,512,4]{1,0,2:T(8,128)} %get-tuple-element.260, f32[4,512]{1,0:T(4,128)S(1)} %maximum_maximum_fusion.2, f32[4]{0:T(128)S(1)} %bitcast.195), kind=kLoop, calls=%fused_computation.5.clone.1 | loop fusion | flops 8386560 | bytes 8405008 | tf_op jit(solution)/shard_map/while/body/eval_jaxpr/reduce_sum | solution.py:182
  141.6 1.4 fusion.93
  143.1 2.1 fusion.95
  145.2 2.0 fusion.96
  148.1 1.2 dynamic_slice.51
  151.7 4.6 %bitcast_reduce_fusion.2 = (f32[4,512]{1,0:T(4,128)S(1)}, f32[1024,512,4]{1,0,2:T(8,128)}) fusion(f32[4]{0:T(128)S(1)} %bitcast.194, bf16[2,1024,4,64]{1,3,2,0:T(8,128)(2,1)S(1)} %get-tuple-element.303, s32[]{:T(128)S(6)} %select_n.121, s32[]{:T(128)S(6)} %select_n.124, bf16[1024,128]{0,1:T(8,128)(2,1)S(1)} %dynamic-slice_bitcast_fusion.4), kind=kOutput, calls=%fused_computation.1.clone.1 | convolution fusion | flops 274724864 | bytes 8790536 | tf_op jit(solution)/shard_map/while/body/eval_jaxpr/qgrd,kgd->grqk/dot_general | solution.py:170
  157.9 1.3 fusion.92
  159.3 5.2 %fusion.94 = f32[4,512]{1,0:T(4,128)S(1)} fusion(f32[1024,512,4]{1,0,2:T(8,128)} %get-tuple-element.260, f32[4,512]{1,0:T(4,128)S(1)} %maximum_maximum_fusion.2, f32[4]{0:T(128)S(1)} %bitcast.195), kind=kLoop, calls=%fused_computation.5.clone.1 | loop fusion | flops 8386560 | bytes 8405008 | tf_op jit(solution)/shard_map/while/body/eval_jaxpr/reduce_sum | solution.py:182
  164.6 1.4 fusion.93
  166.0 2.1 fusion.95
  168.2 2.0 fusion.96
  171.1 1.2 dynamic_slice.51
  174.6 4.6 %bitcast_reduce_fusion.2 = (f32[4,512]{1,0:T(4,128)S(1)}, f32[1024,512,4]{1,0,2:T(8,128)}) fusion(f32[4]{0:T(128)S(1)} %bitcast.194, bf16[2,1024,4,64]{1,3,2,0:T(8,128)(2,1)S(1)} %get-tuple-element.303, s32[]{:T(128)S(6)} %select_n.121, s32[]{:T(128)S(6)} %select_n.124, bf16[1024,128]{0,1:T(8,128)(2,1)S(1)} %dynamic-slice_bitcast_fusion.4), kind=kOutput, calls=%fused_computation.1.clone.1 | convolution fusion | flops 274724864 | bytes 8790536 | tf_op jit(solution)/shard_map/while/body/eval_jaxpr/qgrd,kgd->grqk/dot_general | solution.py:170
  180.8 1.3 fusion.92
  182.2 5.2 %fusion.94 = f32[4,512]{1,0:T(4,128)S(1)} fusion(f32[1024,512,4]{1,0,2:T(8,128)} %get-tuple-element.260, f32[4,512]{1,0:T(4,128)S(1)} %maximum_maximum_fusion.2, f32[4]{0:T(128)S(1)} %bitcast.195), kind=kLoop, calls=%fused_computation.5.clone.1 | loop fusion | flops 8386560 | bytes 8405008 | tf_op jit(solution)/shard_map/while/body/eval_jaxpr/reduce_sum | solution.py:182
  187.5 1.4 fusion.93
  189.0 2.1 fusion.95
  191.1 2.0 fusion.96
  194.0 3.3 %copy.27 = bf16[2,1024,256]{2,0,1:T(2,128)(2,1)} copy(bf16[2,1024,256]{2,1,0:T(8,128)(2,1)} %bitcast.191) | data formatting | bytes 2097152 | tf_op jit(solution)/shard_map/reshape | solution.py:199
  197.3 3.5 %all-to-all-start = ((bf16[2,1024,256]{2,0,1:T(2,128)(2,1)}), bf16[2,1024,256]{2,0,1:T(2,128)(2,1)S(1)}, u32[]{:S(2)}, u32[]{:S(2)}) async-start(bf16[2,1024,256]{2,0,1:T(2,128)(2,1)} %copy.27), calls=%async_computation | async-start | bytes 2097152 | tf_op jit(solution)/shard_map/all_to_all | solution.py:202
  200.8 12.7 %all_gather.15 = f32[3,2048]{1,0:T(4,128)S(1)} all-gather(f32[3,512]{1,0:T(4,128)S(1)} %copy-done.3), channel_id=1, replica_groups=mesh['sp'=4,'tp'=4,'dp'=2] {'tp'}, dimensions={1}, use_global_device_ids=true | all-gather | bytes 30720 | tf_op jit(solution)/shard_map/all_gather | solution.py:96
  213.8 5.8 %multiply_convert_fusion = bf16[2,256,2048]{2,1,0:T(8,128)(2,1)} fusion(bf16[2,256,1024]{2,1,0:T(8,128)(2,1)S(1)} %bitcast.192, bf16[1024,2048]{1,0:T(8,128)(2,1)} %all-gather.2.cloned.1.call-done, f32[2,2048]{1,0:T(2,128)S(1)} %slice.72), kind=kOutput, calls=%fused_computation.58 | convolution fusion | flops 2149580800 | bytes 7356416 | tf_op jit(solution)/shard_map/snc,cd->snd/dot_general | solution.py:203
  (105 shorter events, 15.7 us)
Async XLA Ops:
  6.5 71.2 %copy-start = (bf16[2048,256]{1,0:T(8,128)(2,1)S(1)}, bf16[2048,256]{1,0:T(8,128)(2,1)}, u32[]{:S(2)}) copy-start(bf16[2048,256]{1,0:T(8,128)(2,1)} %param.24) | copy-start | bytes 3145732
  6.5 47.8 %copy-start.6 = (f32[2048]{0:T(1024)S(1)}, f32[2048]{0:T(1024)}, u32[]{:S(2)}) copy-start(f32[2048]{0:T(1024)} %param.20) | copy-start | bytes 24580
  6.5 47.8 %copy-start.5 = (bf16[2048,64]{0,1:T(8,128)(2,1)S(1)}, bf16[2048,64]{0,1:T(8,128)(2,1)}, u32[]{:S(2)}) copy-start(bf16[2048,64]{0,1:T(8,128)(2,1)} %param.25) | copy-start | bytes 786436
  6.5 207.2 %all-gather.2.cloned.1.call-start = ((), (), s32[]{:S(2)}) async-start(), calls=%async_computation.1 | async-start | bytes 5242880 | tf_op jit(solution)/shard_map/all_gather | solution.py:206
  54.4 6.1 %copy-start.4 = (bf16[2048,64]{0,1:T(8,128)(2,1)S(1)}, bf16[2048,64]{0,1:T(8,128)(2,1)}, u32[]{:S(2)}) copy-start(bf16[2048,64]{0,1:T(8,128)(2,1)} %param.26) | copy-start | bytes 786436
  67.5 33.2 %collective-permute-start = (bf16[2,128,128]{1,2,0:T(8,128)(2,1)S(1)}, bf16[2,128,128]{1,2,0:T(8,128)(2,1)S(1)}, u32[]{:S(2)}, u32[]{:S(2)}) collective-permute-start(bf16[2,128,128]{1,2,0:T(8,128)(2,1)S(1)} %get-tuple-element.191), channel_id=1, source_target_pairs={{0,8},{8,16},{16,24},{1,9},{9,17},{17,25},{2,10},{10,18},{18,26},{... | collective-permute-start | bytes 196616 | tf_op jit(solution)/shard_map/ppermute | solution.py:24
  68.8 31.9 %collective-permute-start.1 = (bf16[2,128,128]{1,2,0:T(8,128)(2,1)S(1)}, bf16[2,128,128]{1,2,0:T(8,128)(2,1)S(1)}, u32[]{:S(2)}, u32[]{:S(2)}) collective-permute-start(bf16[2,128,128]{1,2,0:T(8,128)(2,1)S(1)} %get-tuple-element.192), channel_id=1, source_target_pairs={{8,0},{16,8},{24,16},{9,1},{17,9},{25,17},{10,2},{18,10},{26,18},{... | collective-permute-start | bytes 196616 | tf_op jit(solution)/shard_map/ppermute | solution.py:26
  84.4 17.8 %copy-start.1 = (f32[4]{0:T(128)S(1)}, f32[4]{0:T(128)}, u32[]{:S(2)}) copy-start(f32[4]{0:T(128)} %param.29) | copy-start | bytes 52
  84.4 17.8 %copy-start.2 = (f32[4]{0:T(128)S(1)}, f32[4]{0:T(128)}, u32[]{:S(2)}) copy-start(f32[4]{0:T(128)} %param.28) | copy-start | bytes 52
  102.2 98.6 %copy-start.3 = (f32[3,512]{1,0:T(4,128)S(1)}, f32[3,512]{1,0:T(4,128)}, u32[]{:S(2)}) copy-start(f32[3,512]{1,0:T(4,128)} %get-tuple-element.180) | copy-start | bytes 18436
  113.4 6.7 %slice-start = ((s8[8388608]{0:T(1024)(128)(4,1)}), s8[4194304]{0:T(1024)(128)(4,1)S(1)}, s32[]{:S(2)}) async-start(s8[8388608]{0:T(1024)(128)(4,1)} %bitcast.186), calls=%async_computation.2 | async-start | bytes 8388608 | tf_op jit(solution)/shard_map/while
  113.4 6.7 %slice-start.1 = ((s8[8388608]{0:T(1024)(128)(4,1)}), s8[4194304]{0:T(1024)(128)(4,1)S(1)}, s32[]{:S(2)}) async-start(s8[8388608]{0:T(1024)(128)(4,1)} %bitcast.186), calls=%async_computation.3 | async-start | bytes 8388608 | tf_op jit(solution)/shard_map/while
  136.4 6.7 %slice-start = ((s8[8388608]{0:T(1024)(128)(4,1)}), s8[4194304]{0:T(1024)(128)(4,1)S(1)}, s32[]{:S(2)}) async-start(s8[8388608]{0:T(1024)(128)(4,1)} %bitcast.186), calls=%async_computation.2 | async-start | bytes 8388608 | tf_op jit(solution)/shard_map/while
  136.4 6.7 %slice-start.1 = ((s8[8388608]{0:T(1024)(128)(4,1)}), s8[4194304]{0:T(1024)(128)(4,1)S(1)}, s32[]{:S(2)}) async-start(s8[8388608]{0:T(1024)(128)(4,1)} %bitcast.186), calls=%async_computation.3 | async-start | bytes 8388608 | tf_op jit(solution)/shard_map/while
  159.3 6.7 %slice-start = ((s8[8388608]{0:T(1024)(128)(4,1)}), s8[4194304]{0:T(1024)(128)(4,1)S(1)}, s32[]{:S(2)}) async-start(s8[8388608]{0:T(1024)(128)(4,1)} %bitcast.186), calls=%async_computation.2 | async-start | bytes 8388608 | tf_op jit(solution)/shard_map/while
  159.3 6.7 %slice-start.1 = ((s8[8388608]{0:T(1024)(128)(4,1)}), s8[4194304]{0:T(1024)(128)(4,1)S(1)}, s32[]{:S(2)}) async-start(s8[8388608]{0:T(1024)(128)(4,1)} %bitcast.186), calls=%async_computation.3 | async-start | bytes 8388608 | tf_op jit(solution)/shard_map/while
  182.2 6.7 %slice-start = ((s8[8388608]{0:T(1024)(128)(4,1)}), s8[4194304]{0:T(1024)(128)(4,1)S(1)}, s32[]{:S(2)}) async-start(s8[8388608]{0:T(1024)(128)(4,1)} %bitcast.186), calls=%async_computation.2 | async-start | bytes 8388608 | tf_op jit(solution)/shard_map/while
  182.2 6.7 %slice-start.1 = ((s8[8388608]{0:T(1024)(128)(4,1)}), s8[4194304]{0:T(1024)(128)(4,1)S(1)}, s32[]{:S(2)}) async-start(s8[8388608]{0:T(1024)(128)(4,1)} %bitcast.186), calls=%async_computation.3 | async-start | bytes 8388608 | tf_op jit(solution)/shard_map/while
  197.3 16.2 %all-to-all-start = ((bf16[2,1024,256]{2,0,1:T(2,128)(2,1)}), bf16[2,1024,256]{2,0,1:T(2,128)(2,1)S(1)}, u32[]{:S(2)}, u32[]{:S(2)}) async-start(bf16[2,1024,256]{2,0,1:T(2,128)(2,1)} %copy.27), calls=%async_computation | async-start | bytes 2097152 | tf_op jit(solution)/shard_map/all_to_all | solution.py:202
Sparse Core Ops, SparseCore 0:
  70.4 52.5 all-gather.1
where the time goes:
time: 227 us; the launch traced here: 226 us
  matrix products  74.6 us (33%)
  blocking collectives  66.1 us (29%)
  other arithmetic  38.5 us (17%)
  local copies, waits for them, and re-layouts  17.8 us (8%)
  between operations  13.7 us (6%)
  loops' own time  9.49 us (4%)
  starting transfers between devices  6.28 us (3%)
    psum x1, blocking collectives, shards(): lax.psum((jnp.dot(active, w_shift, preferred_element_type=jnp.float32), j...  21.3 us
    reduce_sum x4, other arithmetic, attend(): far_exp.sum(-1, keepdims=True)  21 us
    dot_general x4, matrix products, attend(): jnp.einsum('qgrd,kgd->grqk', q_rows, far_keys, preferred_element_type=jnp...  18.3 us
    all_gather x1, blocking collectives, shards(): lax.all_gather(jnp.concatenate([ctx_keys, ctx_values], axis=-1), 'sp', ax...  15.8 us
    all_gather x1, blocking collectives, shards(): lax.all_gather(gate_part, 'tp', axis=1, tiled=True)  12.7 us
    another operation x1, loops' own time, shards(): lax.map(attend, jnp.arange(samples * blocks, dtype=jnp.int32))  9.49 us
    dot_general x4, matrix products, attend(): jnp.einsum('grqk,kgd->qgrd', (far_exp / normaliser).astype(jnp.bfloat16),...  8.49 us
    all_gather x1, blocking collectives, shards(): lax.all_gather(shift_part, 'tp', axis=1, tiled=True)  8.18 us
  transfers between devices with their start and end apart: 4, of which 0 were waited for; matrix products, arithmetic and copies ran while one was open for 45% of the time, Pallas kernels for 0%

commit v1 on v0

v1 whole, which is shorter than its diff:
```python
import functools

import jax
import jax.numpy as jnp
from jax import lax
from jax.experimental import pallas as pl
from jax.experimental.pallas import tpu as pltpu
from jax.sharding import PartitionSpec as P

HEAD = 64
WINDOW = 128
GRID_COLS = 64
LANES = 128

epsilon = 1e-06
rope_base = 10000.0
masked_value = -1e30
log2e = 1.4426950408889634
MESH = pl.DeviceIdType.MESH


def kernel(
    sizes,
    latent,
    context,
    condition,
    ctx_cond,
    norm_gain,
    w_shift,
    w_scale,
    w_gate,
    w_query,
    w_key,
    w_value,
    w_out,
    sink_logit,
    ctx_lift,
    cosine,
    sine,
    out,
    x_lat,
    x_ctx,
    w_mod,
    w_q,
    w_k,
    w_v,
    w_kv,
    w_o,
    act,
    mod_rx,
    mod_all,
    vec_a,
    vec_b,
    vec_g,
    inv_lat,
    inv_ctx,
    q_buf,
    kv_buf,
    v_buf,
    ckv_buf,
    cv_buf,
    mask_buf,
    att_buf,
    rows_rx,
    ld_sem,
    ma_send,
    ma_recv,
    mb_send,
    mb_recv,
    cx_send,
    cx_recv,
    ha_send,
    ha_recv,
    at_send,
    at_recv,
    wo_send,
    wo_recv,
    wf_send,
    wf_recv,
):
    n_sp, n_tp, n_dp = sizes
    me_sp, me_tp, me_dp = lax.axis_index("sp"), lax.axis_index("tp"), lax.axis_index("dp")
    samples, tokens, width = latent.shape
    ctx_rows = context.shape[1]
    part = w_shift.shape[1]
    heads = w_query.shape[1] // HEAD
    block = tokens // n_tp
    span = block + 2 * WINDOW

    def other(me, step, count):
        return lax.rem(me + step, count)

    barrier = pltpu.get_barrier_semaphore()
    for axis, me, count in (("sp", me_sp, n_sp), ("tp", me_tp, n_tp), ("dp", me_dp, n_dp)):
        for step in range(1, count):
            pl.semaphore_signal(
                barrier, inc=1, device_id={axis: other(me, step, count)}, device_id_type=MESH
            )

    loads = []
    for source, target in (
        (w_shift, w_mod.at[0]),
        (w_scale, w_mod.at[1]),
        (w_gate, w_mod.at[2]),
        (context, x_ctx),
        (latent.at[0], x_lat.at[0]),
        (w_key, w_k),
        (w_value, w_v),
        (w_query, w_q),
        *((latent.at[s], x_lat.at[s]) for s in range(1, samples)),
        (w_out, w_o.at[me_tp]),
    ):
        copy = pltpu.make_async_copy(source, target, ld_sem.at[len(loads)])
        copy.start()
        loads.append(copy)

    act[...] = jnp.zeros_like(act)
    cond = condition[...].astype(jnp.float32)
    act[0:samples, :] = cond / (1.0 + jnp.exp(-cond))
    cond = ctx_cond[...].astype(jnp.float32)
    act[samples : samples + 1, :] = cond / (1.0 + jnp.exp(-cond))
    active = act[...].astype(jnp.bfloat16)
    for i in range(3):
        loads[i].wait()
        mod_rx[me_sp, :, i * part : (i + 1) * part] = jnp.dot(
            active, w_mod[i], preferred_element_type=jnp.float32
        )
    pl.semaphore_wait(barrier, n_sp + n_tp + n_dp - 3)

    def mod_copy(step):
        return pltpu.make_async_remote_copy(
            src_ref=mod_rx.at[me_sp],
            dst_ref=mod_rx.at[me_sp],
            send_sem=ma_send.at[step],
            recv_sem=ma_recv.at[step],
            device_id={"sp": other(me_sp, step, n_sp)},
            device_id_type=MESH,
        )

    for step in range(1, n_sp):
        mod_copy(step).start()

    def inverse_of(rows):
        wide = rows.astype(jnp.float32)
        total = jnp.sum(wide * wide, axis=-1, keepdims=True)
        return jnp.broadcast_to(lax.rsqrt(total / width + epsilon), (rows.shape[0], LANES))

    loads[3].wait()
    for s in range(samples):
        inv_ctx[s] = inverse_of(x_ctx[s])

    def stats(s):
        def body(i, carry):
            rows = pl.ds(pl.multiple_of(i * block, block), block)
            inv_lat[s, rows, :] = inverse_of(x_lat[s, rows, :])
            return carry

        lax.fori_loop(0, n_tp, body, 0)

    loads[4].wait()
    stats(0)
    loads[5].wait()
    loads[6].wait()
    w_kv[...] = jnp.concatenate([w_k[...], w_v[...]], axis=1)

    def wait_mod(step):
        source = other(me_sp, n_sp - step, n_sp)
        pltpu.make_async_remote_copy(
            src_ref=mod_rx.at[source],
            dst_ref=mod_rx.at[source],
            send_sem=ma_send.at[step],
            recv_sem=ma_recv.at[step],
            device_id={"sp": other(me_sp, step, n_sp)},
            device_id_type=MESH,
        ).wait_recv()

    for step in range(1, n_sp):
        wait_mod(step)
    total = mod_rx[0]
    for i in range(1, n_sp):
        total = total + mod_rx[i]
    mod_all[me_tp] = total

    def all_copy(step, source):
        return pltpu.make_async_remote_copy(
            src_ref=mod_all.at[source],
            dst_ref=mod_all.at[source],
            send_sem=mb_send.at[step],
            recv_sem=mb_recv.at[step],
            device_id={"tp": other(me_tp, step, n_tp)},
            device_id_type=MESH,
        )

    for step in range(1, n_tp):
        all_copy(step, me_tp).start()
    for s in range(1, samples):
        loads[7 + s].wait()
        stats(s)
    loads[7].wait()
    for step in range(1, n_tp):
        all_copy(step, other(me_tp, n_tp - step, n_tp)).wait_recv()
    for t in range(n_tp):
        cols = slice(t * part, (t + 1) * part)
        vec_b[:, cols] = mod_all[t, :, 0:part]
        vec_a[:, cols] = (1.0 + mod_all[t, :, part : 2 * part]) * norm_gain[:, cols]
        vec_g[:, cols] = mod_all[t, :, 2 * part : 3 * part]

    share = w_out.shape[0] // n_dp
    mine = pl.ds(pl.multiple_of(me_dp * share, share), share)

    def out_copy(step, source):
        return pltpu.make_async_remote_copy(
            src_ref=w_out.at[mine, :],
            dst_ref=w_o.at[source, mine, :],
            send_sem=wo_send.at[step],
            recv_sem=wo_recv.at[step],
            device_id={"tp": other(me_tp, step, n_tp)},
            device_id_type=MESH,
        )

    def forward_copy(step, hop, part_id):
        source = other(me_tp, n_tp - step, n_tp)
        rows = pl.ds(pl.multiple_of(part_id * share, share), share)
        return pltpu.make_async_remote_copy(
            src_ref=w_o.at[source, rows, :],
            dst_ref=w_o.at[source, rows, :],
            send_sem=wf_send.at[step, hop],
            recv_sem=wf_recv.at[step, hop],
            device_id={"dp": other(me_dp, hop, n_dp)},
            device_id_type=MESH,
        )

    for step in range(1, n_tp):
        out_copy(step, me_tp).start()

    def hidden_of(rows, inverse, row):
        return (
            rows.astype(jnp.float32) * inverse[:, 0:1] * vec_a[row : row + 1, :]
            + vec_b[row : row + 1, :]
        ).astype(jnp.bfloat16)

    def ctx_copy(s, step, source):
        rows = pl.ds(pl.multiple_of(source * ctx_rows, ctx_rows), ctx_rows)
        return pltpu.make_async_remote_copy(
            src_ref=ckv_buf.at[s, rows, :],
            dst_ref=ckv_buf.at[s, rows, :],
            send_sem=cx_send.at[s, step],
            recv_sem=cx_recv.at[s, step],
            device_id={"sp": other(me_sp, step, n_sp)},
            device_id_type=MESH,
        )

    for s in range(samples):
        rows = pl.ds(pl.multiple_of(me_sp * ctx_rows, ctx_rows), ctx_rows)
        ckv_buf[s, rows, :] = jnp.dot(
            hidden_of(x_ctx[s], inv_ctx[s], samples), w_kv[...], preferred_element_type=jnp.float32
        ).astype(jnp.bfloat16)
        for step in range(1, n_sp):
            ctx_copy(s, step, me_sp).start()

    lane = lax.broadcasted_iota(jnp.int32, (block, LANES), 1)
    quarter = HEAD // 4
    first = lane % (2 * quarter) < quarter
    low = lane < HEAD

    def turned(u, cos_rows, sin_rows):
        partner = jnp.where(
            first, pltpu.roll(u, LANES - quarter, 1), pltpu.roll(u, quarter, 1)
        )
        return u * cos_rows + partner * sin_rows

    def project(s):
        def body(i, carry):
            start = pl.multiple_of(i * block, block)
            rows = pl.ds(start, block)
            hid = hidden_of(x_lat[s, rows, :], inv_lat[s, rows, :], s)
            cos_rows, sin_rows = cosine[rows, :], sine[rows, :]
            kv = jnp.dot(hid, w_kv[...], preferred_element_type=jnp.float32)
            kv = jnp.where(low, turned(kv, cos_rows, sin_rows), kv)
            kv_buf[s, pl.ds(pl.multiple_of(start + WINDOW, WINDOW), block), :] = kv.astype(
                jnp.bfloat16
            )
            q = jnp.dot(hid, w_q[...], preferred_element_type=jnp.float32)
            scale = log2e * HEAD ** (-0.5)
            for pair in range(heads // 2):
                u = turned(q[:, pair * LANES : (pair + 1) * LANES], cos_rows, sin_rows) * scale
                q_buf[s, 2 * pair, rows, :] = jnp.where(low, u, 0.0).astype(jnp.bfloat16)
                q_buf[s, 2 * pair + 1, rows, :] = jnp.where(
                    low, pltpu.roll(u, HEAD, 1), 0.0
                ).astype(jnp.bfloat16)
            return carry

        lax.fori_loop(0, n_tp, body, 0)

    def halo_copy(s, side):
        source, target = ((tokens, 0), (WINDOW, WINDOW + tokens))[side]
        step = (1, n_sp - 1)[side]
        return pltpu.make_async_remote_copy(
            src_ref=kv_buf.at[s, pl.ds(source, WINDOW), :],
            dst_ref=kv_buf.at[s, pl.ds(target, WINDOW), :],
            send_sem=ha_send.at[s, side],
            recv_sem=ha_recv.at[s, side],
            device_id={"sp": other(me_sp, step, n_sp)},
            device_id_type=MESH,
        )

    for s in range(samples):
        project(s)
        halo_copy(s, 0).start()
        halo_copy(s, 1).start()

    for s in range(samples):
        for step in range(1, n_sp):
            ctx_copy(s, step, other(me_sp, n_sp - step, n_sp)).wait_recv()
        rows = ckv_buf[s]
        keep = lax.broadcasted_iota(jnp.int32, rows.shape, 1) >= HEAD
        cv_buf[s] = jnp.where(keep, rows.astype(jnp.float32), 1.0).astype(jnp.bfloat16)
    for s in range(samples):
        for side in range(2):
            halo_copy(s, side).wait_recv()
        rows = kv_buf[s]
        keep = lax.broadcasted_iota(jnp.int32, rows.shape, 1) >= HEAD
        v_buf[s] = jnp.where(keep, rows.astype(jnp.float32), 1.0).astype(jnp.bfloat16)

    def rows_copy(s, step, source):
        target = other(me_tp, step, n_tp)
        return pltpu.make_async_remote_copy(
            src_ref=att_buf.at[s, target],
            dst_ref=rows_rx.at[source, s],
            send_sem=at_send.at[s, step],
            recv_sem=at_recv.at[s, step],
            device_id={"tp": target},
            device_id_type=MESH,
        )

    nt = (((1,), (1,)), ((), ()))
    row_id = lax.broadcasted_iota(jnp.int32, (block, span), 0)
    col_id = lax.broadcasted_iota(jnp.int32, (block, span), 1)

    def attend(index, carry):
        s = index // n_tp
        step = index % n_tp + 1
        owner = other(me_tp, step, n_tp)
        start = pl.multiple_of(owner * block, block)
        key_pos = me_sp * tokens + start - WINDOW + col_id
        inside = (
            (key_pos >= 0)
            & (key_pos < n_sp * tokens)
            & (jnp.abs(row_id + WINDOW - col_id) <= WINDOW)
        )
        mask_buf[...] = jnp.where(inside, 0.0, masked_value)
        for h in range(heads):
            q = q_buf[s, h, pl.ds(start, block), :]
            far = lax.dot_general(q, ckv_buf[s], nt, preferred_element_type=jnp.float32)
            near = (
                lax.dot_general(
                    q, kv_buf[s, pl.ds(start, span), :], nt, preferred_element_type=jnp.float32
                )
                + mask_buf[...]
            )
            lift = ctx_lift[h] * log2e
            sink = sink_logit[h] * log2e
            top = jnp.maximum(
                jnp.maximum(
                    jnp.max(near, axis=-1, keepdims=True),
                    jnp.max(far, axis=-1, keepdims=True) + lift,
                ),
                sink,
            )
            near_exp = jnp.exp2(near - top).astype(jnp.bfloat16)
            far_exp = jnp.exp2(far - (top - lift)).astype(jnp.bfloat16)
            both = jnp.dot(
                near_exp, v_buf[s, pl.ds(start, span), :], preferred_element_type=jnp.float32
            ) + jnp.dot(far_exp, cv_buf[s], preferred_element_type=jnp.float32)
            weight = both[:, 0:HEAD] + jnp.exp2(sink - top)
            att_buf[s, owner, :, h * HEAD : (h + 1) * HEAD] = (both[:, HEAD:] / weight).astype(
                jnp.bfloat16
            )

        @pl.when(step < n_tp)
        def _():
            rows_copy(s, step, me_tp).start()

        @pl.when(step == n_tp)
        def _():
            rows_rx[me_tp, s] = att_buf[s, me_tp]

        @pl.when(index == n_tp)
        def _():
            for hop_step in range(1, n_tp):
                out_copy(hop_step, other(me_tp, n_tp - hop_step, n_tp)).wait_recv()
                for hop in range(1, n_dp):
                    forward_copy(hop_step, hop, me_dp).start()

        return carry

    lax.fori_loop(0, samples * n_tp, attend, 0)

    loads[8 + samples - 1].wait()
    for step in range(1, n_tp):
        for hop in range(1, n_dp):
            forward_copy(step, hop, other(me_dp, n_dp - hop, n_dp)).wait_recv()
    chunk = 512
    for s in range(samples):
        for step in range(1, n_tp):
            rows_copy(s, step, other(me_tp, n_tp - step, n_tp)).wait_recv()

        def finish(i, carry):
            cols = pl.ds(pl.multiple_of(i * chunk, chunk), chunk)
            acc = jnp.dot(rows_rx[0, s], w_o[0, :, cols], preferred_element_type=jnp.float32)
            for t in range(1, n_tp):
                acc += jnp.dot(rows_rx[t, s], w_o[t, :, cols], preferred_element_type=jnp.float32)
            out[s, :, cols] = (acc * vec_g[s : s + 1, cols]).astype(jnp.bfloat16)
            return carry

        lax.fori_loop(0, width // chunk, finish, 0)

    for step in range(1, n_sp):
        mod_copy(step).wait_send()
        for s in range(samples):
            ctx_copy(s, step, me_sp).wait_send()
    for s in range(samples):
        halo_copy(s, 0).wait_send()
        halo_copy(s, 1).wait_send()
    for step in range(1, n_tp):
        all_copy(step, me_tp).wait_send()
        out_copy(step, me_tp).wait_send()
        for hop in range(1, n_dp):
            forward_copy(step, hop, me_dp).wait_send()
        for s in range(samples):
            rows_copy(s, step, me_tp).wait_send()


def tables(tokens):
    positions = lax.axis_index("sp") * tokens + jnp.arange(tokens, dtype=jnp.int32)
    lane = jnp.arange(LANES, dtype=jnp.int32)
    quarter = HEAD // 4
    frequency = rope_base ** (-(lane % quarter).astype(jnp.float32) / quarter)
    by_row = lane % HEAD < HEAD // 2
    ticks = jnp.where(by_row, positions[:, None] // GRID_COLS, positions[:, None] % GRID_COLS)
    angles = ticks.astype(jnp.float32) * frequency
    sign = jnp.where(lane % (2 * quarter) < quarter, -1.0, 1.0)
    return jnp.cos(angles), jnp.sin(angles) * sign


def shards(
    latent,
    context,
    condition,
    ctx_cond,
    norm_gain,
    w_shift,
    w_scale,
    w_gate,
    w_query,
    w_key,
    w_value,
    w_out,
    sink_logit,
    ctx_lift,
):
    samples, tokens, width = latent.shape
    ctx_rows = context.shape[1]
    n_sp, n_tp, n_dp = lax.axis_size("sp"), lax.axis_size("tp"), lax.axis_size("dp")
    heads = w_query.shape[1] // HEAD
    assert w_key.shape[1] == HEAD and samples < 8 and heads % 2 == 0
    part = w_shift.shape[1]
    block = tokens // n_tp
    cosine, sine = tables(tokens)
    bf16, f32 = jnp.bfloat16, jnp.float32
    vmem = pl.BlockSpec(memory_space=pltpu.VMEM)
    smem = pl.BlockSpec(memory_space=pltpu.SMEM)
    anywhere = pl.BlockSpec(memory_space=pl.ANY)
    dma = pltpu.SemaphoreType.DMA
    padded = tokens + 2 * WINDOW
    return pl.pallas_call(
        functools.partial(kernel, (n_sp, n_tp, n_dp)),
        out_shape=jax.ShapeDtypeStruct((samples, block, width), bf16),
        in_specs=[
            anywhere,
            anywhere,
            vmem,
            vmem,
            vmem,
            anywhere,
            anywhere,
            anywhere,
            anywhere,
            anywhere,
            anywhere,
            anywhere,
            smem,
            smem,
            vmem,
            vmem,
        ],
        out_specs=vmem,
        scratch_shapes=[
            pltpu.VMEM(latent.shape, bf16),
            pltpu.VMEM(context.shape, bf16),
            pltpu.VMEM((3,) + w_shift.shape, bf16),
            pltpu.VMEM(w_query.shape, bf16),
            pltpu.VMEM(w_key.shape, bf16),
            pltpu.VMEM(w_value.shape, bf16),
            pltpu.VMEM((width, 2 * HEAD), bf16),
            pltpu.VMEM((n_tp,) + w_out.shape, bf16),
            pltpu.VMEM((8, w_shift.shape[0]), f32),
            pltpu.VMEM((n_sp, 8, 3 * part), f32),
            pltpu.VMEM((n_tp, 8, 3 * part), f32),
            pltpu.VMEM((8, width), f32),
            pltpu.VMEM((8, width), f32),
            pltpu.VMEM((8, width), f32),
            pltpu.VMEM((samples, tokens, LANES), f32),
            pltpu.VMEM((samples, ctx_rows, LANES), f32),
            pltpu.VMEM((samples, heads, tokens, LANES), bf16),
            pltpu.VMEM((samples, padded, LANES), bf16),
            pltpu.VMEM((samples, padded, LANES), bf16),
            pltpu.VMEM((samples, n_sp * ctx_rows, LANES), bf16),
            pltpu.VMEM((samples, n_sp * ctx_rows, LANES), bf16),
            pltpu.VMEM((block, block + 2 * WINDOW), f32),
            pltpu.VMEM((samples, n_tp, block, heads * HEAD), bf16),
            pltpu.VMEM((n_tp, samples, block, heads * HEAD), bf16),
            dma((8 + samples,)),
            dma((n_sp,)),
            dma((n_sp,)),
            dma((n_tp,)),
            dma((n_tp,)),
            dma((samples, n_sp)),
            dma((samples, n_sp)),
            dma((samples, 2)),
            dma((samples, 2)),
            dma((samples, n_tp)),
            dma((samples, n_tp)),
            dma((n_tp,)),
            dma((n_tp,)),
            dma((n_tp, n_dp)),
            dma((n_tp, n_dp)),
        ],
        compiler_params=pltpu.CompilerParams(
            collective_id=0, has_side_effects=True, vmem_limit_bytes=60 * 1024 * 1024
        ),
    )(
        latent,
        context,
        condition,
        ctx_cond.reshape(1, -1),
        norm_gain.reshape(1, -1),
        w_shift,
        w_scale,
        w_gate,
        w_query,
        w_key,
        w_value,
        w_out,
        sink_logit,
        ctx_lift,
        cosine,
        sine,
    )


def solution(mesh):
    return jax.shard_map(
        shards,
        mesh=mesh,
        in_specs=(
            P("dp", "sp", None),
            P("dp", "sp", None),
            P("dp", "sp"),
            P("sp"),
            P(),
            P("sp", "tp"),
            P("sp", "tp"),
            P("sp", "tp"),
            P(None, "tp"),
            P(None, "tp"),
            P(None, "tp"),
            P("tp", None),
            P("tp"),
            P("tp"),
        ),
        out_specs=P("dp", ("sp", "tp"), None),
        check_vma=False,
    )
```

time: 227 us -> 72.3 us (0.32)
  the two profiles are of different devices: /device:TPU:0 before, /device:TPU:28 now
where the time goes in v1:
time: 72.3 us; the launch traced here: 72 us
  Pallas kernels  60.6 us (84%)
  local copies, waits for them, and re-layouts  8.31 us (11%)
  other arithmetic  3.13 us (4%)
    pallas_call x1, Pallas kernels, shards(): pl.pallas_call(functools.partial(kernel, (n_sp, n_tp, n_dp)), out_shape=j...  60.6 us
    unnamed x3, local copies, waits for them, and re-layouts  7.06 us
    mul x1, other arithmetic, tables(): return (jnp.cos(angles), jnp.sin(angles) * sign)  3.11 us

profile of v1, /device:TPU:28, one launch (start us, length us, event | category | flops | bytes accessed | tf_op | source)
XLA Modules:
  0.0 72.0 jit_solution(7156169601778167796)
XLA Ops:
  0.0 1.2 %reshape.86.ctx_cond = bf16[1,512]{1,0:T(2,128)(2,1)} reshape(bf16[512]{0:T(512)(128)(2,1)} %param.17) | data formatting | bytes 2048 | tf_op jit(solution)/shard_map/reshape | solution.py:546
  1.3 2.0 %copy.15.w_key = bf16[2048,64]{1,0:T(8,128)(2,1)} copy(bf16[2048,64]{0,1:T(8,128)(2,1)} %param.23) | data formatting | bytes 524288 | tf_op args[9]
  3.2 1.9 %copy.16.w_value = bf16[2048,64]{1,0:T(8,128)(2,1)} copy(bf16[2048,64]{0,1:T(8,128)(2,1)} %param.24) | data formatting | bytes 524288 | tf_op args[10]
  5.2 3.1 %sine_multiply_fusion = (f32[1024,128]{1,0:T(8,128)}, f32[1024,128]{1,0:T(8,128)}) fusion(f32[128]{0:T(128)S(1)} %get-tuple-element.9, f32[128]{0:T(128)S(1)} %get-tuple-element.10, s32[1024]{0:T(1024)S(1)} %get-tuple-element.7, s32[1024]{0:T(1024)S(1)} %get-tuple-element.8, pred[128]{0:T(512)(128)(4,1)S(1)} %fusion.6), kind=kLoop, calls=%fused_computation | loop fusion | flops 524288 | bytes 1057920 | tf_op jit(solution)/shard_map/mul | solution.py:443
  8.3 60.6 %shard_map.136 = bf16[2,256,2048]{2,1,0:T(8,128)(2,1)} custom-call(bf16[2,1024,2048]{2,1,0:T(8,128)(2,1)} %latent.1, bf16[2,256,2048]{2,1,0:T(8,128)(2,1)} %context.1, bf16[2,512]{1,0:T(2,128)(2,1)} %condition.1, bf16[1,512]{1,0:T(2,128)(2,1)} %reshape.86.ctx_cond, f32[1,2048]{1,0:T(1,128)} %bitcast.1, bf16[512,512]{1,0:T(8,128)(2,1)} %w_shift.1, ...), custom_call_target="tpu_custom_call" | custom-call | tf_op jit(solution)/shard_map/pallas_call | solution.py:476
  68.9 3.2 %copy.18 = bf16[2,256,2048]{2,1,0:T(8,128)(2,1)} copy(bf16[2,256,2048]{2,1,0:T(8,128)(2,1)} %shard_map.136) | data formatting | bytes 4194304
  (3 shorter events, 0.0 us)
